TPU v7x, 32 devices: a whole 2x2x4 slice. The times are simulated.
32 devices in a mesh: kv: 8 (over z, y), tp: 4 (over x, core).
Axes of the slice: x: 2, y: 2, z: 4, core: 2. Of those that a mesh axis runs over, the one named last changes fastest.
Arguments:
- tokens: bfloat16 [256, 4096], P(None, ('kv', 'tp')), may hold values from -60 to 60
- past_state: float32 [256, 16, 128, 128], P('kv', 'tp'), may hold values from -4 to 4
- pre_gain: float32 [4096], replicated, may hold values from 0.1 to 1.9
- pre_gate: bfloat16 [4096, 11264], P(None, ('kv', 'tp')), may hold values from -0.09375 to 0.09375
- pre_up: bfloat16 [4096, 11264], P(None, ('kv', 'tp')), may hold values from -0.09375 to 0.09375
- pre_down: bfloat16 [11264, 4096], P(('kv', 'tp')), may hold values from -0.109375 to 0.109375
- mix_gain: float32 [4096], replicated, may hold values from 0.1 to 1.9
- query_weight: bfloat16 [4096, 2048], P('kv', 'tp'), may hold values from -0.09375 to 0.09375
- forget_weight: bfloat16 [4096, 2048], P('kv', 'tp'), may hold values from -0.09375 to 0.09375
- value_weight: bfloat16 [4096, 2048], P('kv', 'tp'), may hold values from -0.09375 to 0.09375
- output_gate_weight: bfloat16 [4096, 2048], P('kv', 'tp'), may hold values from -0.09375 to 0.09375
- forget_floor: float32 [2048], P('tp'), may hold values from 0.02 to 0.9
- head_gain: float32 [128], replicated, may hold values from 0.1 to 1.9
- proj_out: bfloat16 [2048, 4096], P('tp', 'kv'), may hold values from -0.125 to 0.125
- post_gain: float32 [4096], replicated, may hold values from 0.1 to 1.9
- post_gate: bfloat16 [4096, 11264], P(None, ('kv', 'tp')), may hold values from -0.09375 to 0.09375
- post_up: bfloat16 [4096, 11264], P(None, ('kv', 'tp')), may hold values from -0.09375 to 0.09375
- post_down: bfloat16 [11264, 4096], P(('kv', 'tp')), may hold values from -0.109375 to 0.109375
Outputs:
- result: bfloat16 [256, 4096], P(None, ('kv', 'tp'))
- new_state: float32 [256, 16, 128, 128], P('kv', 'tp')
All inputs are finite; a program needn't handle non-finite values.
Results may differ from a plain program's by a relative error of at most 0.014.
Values may be sent and summed in bfloat16 or wider, within the bound.
A program may use at most 128 MiB of HBM per device.

v0:
```python
import jax
import jax.numpy as jnp
from jax import lax
from jax.sharding import PartitionSpec as P

D = 4096


epsilon = 1e-06


def half_inputs(activations, gain, w_gate, w_up):
    piece_float = lax.all_gather(activations, ("kv", "tp"), axis=1, tiled=True).astype(jnp.float32)
    normed = (piece_float * gain).astype(jnp.bfloat16)
    gate_acc = jnp.dot(normed, w_gate, preferred_element_type=jnp.float32)
    up_acc = jnp.dot(normed, w_up, preferred_element_type=jnp.float32)
    squares = jnp.sum(piece_float * piece_float, axis=1)
    row_scale = lax.rsqrt(squares / D + epsilon)[:, None]
    return (jax.nn.silu(row_scale * gate_acc) * (row_scale * up_acc)).astype(jnp.bfloat16)


def down_sum(hidden, w_down):
    return lax.psum_scatter(
        jnp.dot(hidden, w_down, preferred_element_type=jnp.float32),
        ("kv", "tp"),
        scatter_dimension=1,
        tiled=True,
    )


def per_device(
    tokens,
    past_state,
    pre_gain,
    pre_gate,
    pre_up,
    pre_down,
    mix_gain,
    query_weight,
    forget_weight,
    value_weight,
    output_gate_weight,
    forget_floor,
    head_gain,
    proj_out,
    post_gain,
    post_gate,
    post_up,
    post_down,
):
    whole_rows = lax.all_gather(tokens, ("kv", "tp"), axis=1, tiled=True)
    whole_float = whole_rows.astype(jnp.float32)
    row_scale = lax.rsqrt(jnp.mean(whole_float * whole_float, axis=1, keepdims=True) + epsilon)
    normed = (whole_float * pre_gain).astype(jnp.bfloat16)
    gate_pre = row_scale * jnp.dot(normed, pre_gate, preferred_element_type=jnp.float32)
    up_pre = row_scale * jnp.dot(normed, pre_up, preferred_element_type=jnp.float32)
    hidden = (jax.nn.silu(gate_pre) * up_pre).astype(jnp.bfloat16)
    kv_sums = lax.psum_scatter(
        jnp.dot(hidden, pre_down, preferred_element_type=jnp.float32).astype(jnp.bfloat16),
        "kv",
        scatter_dimension=1,
        tiled=True,
    )
    block_sum = lax.psum(kv_sums, "tp").astype(jnp.float32)
    block_width = block_sum.shape[1]
    block_old = lax.dynamic_slice_in_dim(
        whole_rows, lax.axis_index("kv") * block_width, block_width, 1
    )
    block_rows = (block_old.astype(jnp.float32) + 0.5 * block_sum).astype(jnp.bfloat16)
    own_width = block_width // lax.axis_size("tp")
    after_first = lax.dynamic_slice_in_dim(
        block_rows, lax.axis_index("tp") * own_width, own_width, 1
    )
    block_width = block_rows.shape[1]
    block_float = block_rows.astype(jnp.float32)
    block_gain = lax.dynamic_slice_in_dim(
        mix_gain, lax.axis_index("kv") * block_width, block_width, 0
    )
    squares = lax.psum(jnp.sum(block_float * block_float, axis=1), "kv")
    normed = (block_float * block_gain).astype(jnp.bfloat16)
    own_rows = past_state.shape[0]
    weight_list = (query_weight, forget_weight, value_weight, output_gate_weight)
    projected = lax.psum_scatter(
        jnp.concatenate(
            [
                jnp.dot(normed, weight_part, preferred_element_type=jnp.float32)
                for weight_part in weight_list
            ],
            axis=1,
        ).astype(jnp.bfloat16),
        "kv",
        scatter_dimension=0,
        tiled=True,
    ).astype(jnp.float32)
    own_squares = lax.dynamic_slice_in_dim(squares, lax.axis_index("kv") * own_rows, own_rows, 0)
    projected = projected * lax.rsqrt(own_squares / D + epsilon)[:, None]
    pre_query, pre_forget, pre_value, pre_gate_out = jnp.split(projected, 4, axis=1)
    local_heads = past_state.shape[1]
    head_width = past_state.shape[2]
    head_shape = (own_rows, local_heads, head_width)
    floors = forget_floor.reshape(local_heads, head_width)
    forget_heads = pre_forget.reshape(head_shape)
    forget = floors + (1.0 - floors) * jax.nn.sigmoid(forget_heads)
    written = (1.0 - floors) * jax.nn.sigmoid(-forget_heads)
    query_act = jax.nn.silu(pre_query.reshape(head_shape))
    value_act = pre_value.reshape(head_shape)
    new_state = (
        forget[:, :, :, None] * past_state + written[:, :, :, None] * value_act[:, :, None, :]
    )
    readout = jnp.einsum("bhkv,bhk->bhv", new_state, query_act, precision=lax.Precision.HIGHEST)
    readout = (
        readout
        * lax.rsqrt(jnp.mean(readout * readout, axis=2, keepdims=True) + epsilon)
        * head_gain
    )
    mixed_in = (
        readout.reshape(own_rows, local_heads * head_width) * jax.nn.silu(pre_gate_out)
    ).astype(jnp.bfloat16)
    partials = jnp.dot(
        lax.all_gather(mixed_in, "kv", axis=0, tiled=True),
        proj_out,
        preferred_element_type=jnp.float32,
    ).astype(jnp.bfloat16)
    mixed_sum = lax.psum_scatter(partials, "tp", scatter_dimension=1, tiled=True).astype(
        jnp.float32
    )
    second = (after_first.astype(jnp.float32) + mixed_sum).astype(jnp.bfloat16)
    hidden_two = half_inputs(second, post_gain, post_gate, post_up)
    result = (second.astype(jnp.float32) + 0.5 * down_sum(hidden_two, post_down)).astype(
        jnp.bfloat16
    )
    return (result, new_state)


def solution(mesh):
    placed = (
        P(None, ("kv", "tp")),
        P("kv", "tp", None, None),
        P(),
        P(None, ("kv", "tp")),
        P(None, ("kv", "tp")),
        P(("kv", "tp"), None),
        P(),
        P("kv", "tp"),
        P("kv", "tp"),
        P("kv", "tp"),
        P("kv", "tp"),
        P("tp"),
        P(),
        P("tp", "kv"),
        P(),
        P(None, ("kv", "tp")),
        P(None, ("kv", "tp")),
        P(("kv", "tp"), None),
    )
    return jax.shard_map(
        per_device,
        mesh=mesh,
        in_specs=placed,
        out_specs=(P(None, ("kv", "tp")), P("kv", "tp", None, None)),
        check_vma=False,
    )
```

profile of v0, /device:TPU:0, one launch (start us, length us, event | category | flops | bytes accessed | tf_op | source)
XLA Modules:
  0.0 548.7 jit_solution(15226853268982632663)
XLA Ops:
  7.2 0.0 copy-start
  7.2 0.0 all-gather.3.cloned.1.call-start
  7.2 0.7 all-gather.3.cloned.1.call-update
  7.9 0.0 reduce-scatter.7.cloned.1.call-start
  8.0 58.6 %all-gather.3.cloned.1.call-done = bf16[256,4096]{1,0:T(8,128)(2,1)} async-done(((bf16[256,128]{1,0:T(8,128)(2,1)}), bf16[256,4096]{1,0:T(8,128)(2,1)}) %all-gather.3.cloned.1.call-update) | async-done | bytes 2097168 | tf_op jit(solution)/shard_map/all_gather | solution.py:51
  66.6 2.1 fusion
  68.7 0.0 copy-start.7
  68.7 3.4 fusion.12
  72.1 0.0 copy-done
  72.1 0.0 copy-done.7
  72.1 7.5 %convolution_convert_fusion = bf16[256,4096]{1,0:T(8,128)(2,1)} fusion(bf16[352,4096]{1,0:T(8,128)(2,1)S(1)} %copy-done, bf16[4096,352]{0,1:T(8,128)(2,1)} %param.22, bf16[256,4096]{1,0:T(8,128)(2,1)} %all-gather.3.cloned.1.call-done, f32[4096]{0:T(1024)S(1)} %copy-done.7, f32[256,352]{0,1:T(8,128)S(1)} %fusion.12, f32[256]{0:T(256)S(1)} %add_rsqrt_fusion.2), kind=kOutput, calls=%fused_computation.5 | convolution fusion | flops 1481220096 | bytes 10339328 | tf_op jit(solution)/shard_map/dot_general | solution.py:59
  79.6 0.0 reduce-scatter.7.cloned.1.call-update
  79.6 0.0 all-reduce.2.cloned.1.call-start
  79.7 68.1 %reduce-scatter.7.cloned.1.call-done = bf16[256,512]{1,0:T(8,128)(2,1)} async-done(((bf16[256,4096]{1,0:T(8,128)(2,1)}), bf16[256,512]{1,0:T(8,128)(2,1)}) %reduce-scatter.7.cloned.1.call-update) | async-done | bytes 262160 | tf_op jit(solution)/shard_map/reduce_scatter | solution.py:58
  147.8 0.0 all-reduce.2.cloned.1.call-update
  147.8 0.0 reduce-scatter.9.cloned.1.call-start
  147.8 0.8 dynamic_slice.14
  148.6 32.8 %all-reduce.2.cloned.1.call-done = bf16[256,512]{1,0:T(8,128)(2,1)} async-done(((bf16[256,512]{1,0:T(8,128)(2,1)}), bf16[256,512]{1,0:T(8,128)(2,1)}) %all-reduce.2.cloned.1.call-update) | async-done | bytes 262160 | tf_op jit(solution)/shard_map/psum | solution.py:64
  181.4 1.2 fusion.42
  182.6 1.3 convolution_convert_fusion.3
  183.9 1.3 convolution_convert_fusion.2
  185.3 0.0 copy-start.5
  185.3 1.3 convolution_convert_fusion.4
  186.6 1.3 convolution_convert_fusion.5
  188.0 1.1 pad_maximum_fusion
  189.1 0.0 reduce-scatter.9.cloned.1.call-update
  189.1 0.0 reduce-scatter.13.cloned.1.call-start
  189.2 0.0 copy-done.5
  189.2 21.6 %psum.15 = f32[256]{0:T(256)S(1)} all-reduce(f32[256]{0:T(256)S(1)} %get-tuple-element.2), channel_id=1, replica_groups=mesh['kv'=8,'tp'=4] {'kv'}, use_global_device_ids=true, to_apply=%region_5.6 | all-reduce | flops 256 | bytes 2048 | tf_op jit(solution)/shard_map/psum | solution.py:79
  210.8 0.1 add_rsqrt_fusion.3
  210.8 42.6 %reduce-scatter.9.cloned.1.call-done = bf16[32,2048]{1,0:T(8,128)(2,1)} async-done(((bf16[256,2048]{1,0:T(8,128)(2,1)}), bf16[32,2048]{1,0:T(8,128)(2,1)}) %reduce-scatter.9.cloned.1.call-update) | async-done | bytes 131088 | tf_op jit(solution)/shard_map/reduce_scatter | solution.py:83
  253.5 1.0 convert_multiply_fusion.6
  254.5 0.7 fusion.64
  255.1 0.6 reshape.74
  255.8 0.9 divide_multiply_fusion
  256.7 0.6 div.65
  257.3 0.9 mul.203
  258.2 1.5 div.63
  259.6 0.9 multiply_add_fusion.1
  260.5 8.2 %multiply_add_fusion = f32[32,4,128,128]{3,2,1,0:T(8,128)S(1)} fusion(f32[32,4,128,128]{3,2,1,0:T(8,128)} %param.19, f32[32,4,128]{2,1,0:T(4,128)S(1)} %mul.203, f32[32,4,128]{2,1,0:T(4,128)S(1)} %bitcast.39, f32[32,4,128]{2,1,0:T(4,128)S(1)} %bitcast.38), kind=kLoop, calls=%fused_computation | loop fusion | flops 6291456 | bytes 16973824 | tf_op jit(solution)/shard_map/add | solution.py:108
  268.8 0.0 copy-start.1
  268.8 0.0 copy-start.6
  268.8 0.0 copy-start.3
  268.8 7.2 %fusion.65 = f32[32,4,1,128]{3,2,1,0:T(1,128)S(1)} fusion(f32[32,4,128,128]{3,2,1,0:T(8,128)S(1)} %multiply_add_fusion, f32[32,4,128,1]{2,3,1,0:T(1,128)S(1)} %bitcast.37), kind=kOutput, calls=%fused_computation.68 | convolution fusion | flops 25165824 | bytes 8519680 | tf_op jit(solution)/shard_map/bhkv,bhk->bhv/dot_general | solution.py:110
  276.0 0.0 copy-done.1
  276.0 0.1 multiply_reduce_fusion
  276.1 0.1 multiply_multiply_fusion
  276.3 30.8 %all_gather.10 = bf16[256,512]{1,0:T(8,128)(2,1)S(1)} all-gather(bf16[32,512]{1,0:T(8,128)(2,1)S(1)} %fusion.61), channel_id=1, replica_groups=mesh['kv'=8,'tp'=4] {'kv'}, dimensions={0}, use_global_device_ids=true | all-gather | bytes 294912 | tf_op jit(solution)/shard_map/all_gather | solution.py:120
  307.1 0.3 convolution_convert_fusion.1
  307.4 0.8 copy.22
  308.3 0.0 reduce-scatter.13.cloned.1.call-update
  308.3 0.0 all-gather.5.cloned.1.call-start
  308.3 19.2 %reduce-scatter.13.cloned.1.call-done = bf16[128,256]{1,0:T(8,128)(2,1)} async-done(((bf16[512,256]{1,0:T(8,128)(2,1)}), bf16[128,256]{1,0:T(8,128)(2,1)}) %reduce-scatter.13.cloned.1.call-update) | async-done | bytes 65552
  327.5 0.9 copy.23
  328.5 0.7 add_convert_fusion.2
  329.1 0.0 all-gather.5.cloned.1.call-update
  329.1 0.3 reduce-scatter.11.cloned.1.call-start
  329.4 54.4 %all-gather.5.cloned.1.call-done = bf16[256,4096]{1,0:T(8,128)(2,1)} async-done(((bf16[256,128]{1,0:T(8,128)(2,1)}), bf16[256,4096]{1,0:T(8,128)(2,1)}) %all-gather.5.cloned.1.call-update) | async-done | bytes 2097168 | tf_op jit(solution)/shard_map/all_gather | solution.py:13
  383.8 2.1 fusion.2
  385.9 3.4 fusion.18
  389.3 8.9 %fusion.37 = f32[256,4096]{1,0:T(8,128)} fusion(bf16[352,4096]{1,0:T(8,128)(2,1)} %param.35, bf16[4096,352]{0,1:T(8,128)(2,1)} %param.34, bf16[256,4096]{1,0:T(8,128)(2,1)} %all-gather.5.cloned.1.call-done, f32[4096]{0:T(1024)S(1)} %copy-done.4, f32[256,352]{0,1:T(8,128)S(1)} %fusion.18, f32[256]{0:T(256)S(1)} %add_rsqrt_fusion.1), kind=kOutput, calls=%fused_computation.27 | convolution fusion | flops 1480171520 | bytes 12436480 | tf_op jit(solution)/shard_map/dot_general | solution.py:24
  398.2 0.0 reduce-scatter.11.cloned.1.call-update
  398.3 142.1 %reduce-scatter.11.cloned.1.call-done = f32[256,128]{1,0:T(8,128)} async-done(((f32[256,4096]{1,0:T(8,128)}), f32[256,128]{1,0:T(8,128)}) %reduce-scatter.11.cloned.1.call-update) | async-done | bytes 131088 | tf_op jit(solution)/shard_map/reduce_scatter | solution.py:23
  540.3 1.6 add_convert_fusion.1
  (13 shorter events, 0.1 us)
Async XLA Ops:
  7.2 65.0 %copy-start = (bf16[352,4096]{1,0:T(8,128)(2,1)S(1)}, bf16[352,4096]{1,0:T(8,128)(2,1)}, u32[]{:S(2)}) copy-start(bf16[352,4096]{1,0:T(8,128)(2,1)} %param.23) | copy-start | bytes 8650756
  7.2 59.4 %all-gather.3.cloned.1.call-start = ((), (), s32[]{:S(2)}) async-start(), calls=%async_computation.4 | async-start | bytes 2162688 | tf_op jit(solution)/shard_map/all_gather | solution.py:51
  7.9 139.8 %reduce-scatter.7.cloned.1.call-start = ((), (), s32[]{:S(2)}) async-start(), calls=%async_computation.5 | async-start | bytes 2359296 | tf_op jit(solution)/shard_map/reduce_scatter | solution.py:58
  68.7 3.5 copy-start.7
  79.6 101.7 %all-reduce.2.cloned.1.call-start = ((), (), s32[]{:S(2)}) async-start(), calls=%async_computation.6 | async-start | bytes 524288 | tf_op jit(solution)/shard_map/psum | solution.py:64
  147.8 105.7 %reduce-scatter.9.cloned.1.call-start = ((), (), s32[]{:S(2)}) async-start(), calls=%async_computation.7 | async-start | bytes 1179648 | tf_op jit(solution)/shard_map/reduce_scatter | solution.py:83
  185.3 3.9 copy-start.5
  189.1 138.4 %reduce-scatter.13.cloned.1.call-start = ((), (), s32[]{:S(2)}) async-start(), calls=%async_computation.10 | async-start | bytes 327680
  268.8 7.2 %copy-start.1 = (f32[32,4,128,128]{3,2,1,0:T(8,128)}, f32[32,4,128,128]{3,2,1,0:T(8,128)S(1)}, u32[]{:S(2)}) copy-start(f32[32,4,128,128]{3,2,1,0:T(8,128)S(1)} %multiply_add_fusion) | copy-start | bytes 25165828
  268.8 7.3 %copy-start.6 = (f32[128]{0:T(128)S(1)}, f32[128]{0:T(128)}, u32[]{:S(2)}) copy-start(f32[128]{0:T(128)} %param.30) | copy-start | bytes 1540
  268.8 38.3 %copy-start.3 = (bf16[512,512]{1,0:T(8,128)(2,1)S(1)}, bf16[512,512]{1,0:T(8,128)(2,1)}, u32[]{:S(2)}) copy-start(bf16[512,512]{1,0:T(8,128)(2,1)} %param.31) | copy-start | bytes 1572868
  276.0 109.9 %copy-start.4 = (f32[4096]{0:T(1024)S(1)}, f32[4096]{0:T(1024)}, u32[]{:S(2)}) copy-start(f32[4096]{0:T(1024)} %param.32) | copy-start | bytes 49156
  308.3 75.5 %all-gather.5.cloned.1.call-start = ((), (), s32[]{:S(2)}) async-start(), calls=%async_computation.8 | async-start | bytes 2162688 | tf_op jit(solution)/shard_map/all_gather | solution.py:13
  329.1 211.2 %reduce-scatter.11.cloned.1.call-start = ((), (), s32[]{:S(2)}) async-start(), calls=%async_computation.9 | async-start | bytes 4325376 | tf_op jit(solution)/shard_map/reduce_scatter | solution.py:23
  398.2 142.1 %copy-start.2 = (bf16[256,128]{1,0:T(8,128)(2,1)S(1)}, bf16[256,128]{1,0:T(8,128)(2,1)}, u32[]{:S(2)}) copy-start(bf16[256,128]{1,0:T(8,128)(2,1)} %add_convert_fusion.2) | copy-start | bytes 196612
Sparse Core Ops, SparseCore 0:
  10.8 55.6 all-gather.2
  79.7 67.9 reduce-scatter.6
  150.1 31.2 all-reduce.1
  189.2 64.1 reduce-scatter.8
  308.4 19.0 reduce-scatter.12
  330.8 52.9 all-gather.4
  398.4 141.8 reduce-scatter.10
where the time goes:
time: 550 us; the launch traced here: 549 us
  waiting for transfers between devices  418 us (76%)
  blocking collectives  52.4 us (10%)
  matrix products  36.1 us (7%)
  other arithmetic  20.7 us (4%)
  between operations  14.4 us (3%)
  local copies, waits for them, and re-layouts  6.21 us (1%)
    reduce_scatter x1, waiting for transfers between devices, down_sum(): lax.psum_scatter(jnp.dot(hidden, w_down, preferred_element_type=jnp.float...  142 us
    reduce_scatter x1, waiting for transfers between devices, per_device(): lax.psum_scatter(jnp.dot(hidden, pre_down, preferred_element_type=jnp.flo...  68.1 us
    all_gather x1, waiting for transfers between devices, per_device(): whole_rows = lax.all_gather(tokens, ('kv', 'tp'), axis=1, tiled=True)  58.6 us
    all_gather x1, waiting for transfers between devices, half_inputs(): lax.all_gather(activations, ('kv', 'tp'), axis=1, tiled=True)  54.4 us
    reduce_scatter x1, waiting for transfers between devices, per_device(): lax.psum_scatter(jnp.concatenate([jnp.dot(normed, weight_part, preferred_...  42.6 us
    psum x1, waiting for transfers between devices, per_device(): block_sum = lax.psum(kv_sums, 'tp').astype(jnp.float32)  32.8 us
    all_gather x1, blocking collectives, per_device(): lax.all_gather(mixed_in, 'kv', axis=0, tiled=True)  30.8 us
    psum x1, blocking collectives, per_device(): squares = lax.psum(jnp.sum(block_float * block_float, axis=1), 'kv')  21.6 us
  transfers between devices with their start and end apart: 7, of which 7 were waited for; matrix products, arithmetic and copies ran while one was open for 0% of the time, Pallas kernels for 0%

commit v1 on v0

--- a/solution.py
+++ b/solution.py
@@ -1,6 +1,10 @@
+import functools
+
 import jax
 import jax.numpy as jnp
 from jax import lax
+from jax.experimental import pallas as pl
+from jax.experimental.pallas import tpu as pltpu
 from jax.sharding import PartitionSpec as P
 
 D = 4096
@@ -28,7 +32,7 @@
     )
 
 
-def per_device(
+def per_device_plain(
     tokens,
     past_state,
     pre_gain,
@@ -132,6 +136,440 @@
     return (result, new_state)
 
 
+LANES = 128
+CORES = 2
+F32, BF16 = jnp.float32, jnp.bfloat16
+MESH = pl.DeviceIdType.MESH
+
+
+class Grid:
+    def __init__(self, n_kv, n_tp):
+        self.nk, self.nt, self.nx = n_kv, n_tp, n_tp // CORES
+        self.kv, self.tp = lax.axis_index("kv"), lax.axis_index("tp")
+        self.x, self.c = self.tp // CORES, self.tp % CORES
+        self.oc = 1 - self.c
+
+    def k(self, step):
+        return lax.rem(self.kv + step, self.nk)
+
+    def xi(self, step):
+        return lax.rem(self.x + step, self.nx)
+
+    def t(self, step):
+        return lax.rem(self.tp + step, self.nt)
+
+    def block(self, k, x, c):
+        return k * self.nt + x * CORES + c
+
+
+def remote(src, dst, send, recv, k, t):
+    return pltpu.make_async_remote_copy(
+        src_ref=src, dst_ref=dst, send_sem=send, recv_sem=recv,
+        device_id={"kv": k, "tp": t}, device_id_type=MESH,
+    )
+
+
+def barrier(g):
+    sem = pltpu.get_barrier_semaphore()
+    for step in range(1, g.nk):
+        pl.semaphore_signal(sem, inc=1, device_id={"kv": g.k(step), "tp": g.tp}, device_id_type=MESH)
+    for step in range(1, g.nt):
+        pl.semaphore_signal(sem, inc=1, device_id={"kv": g.kv, "tp": g.t(step)}, device_id_type=MESH)
+    pl.semaphore_wait(sem, g.nk - 1 + g.nt - 1)
+
+
+def cols(ref, block, width=LANES):
+    return ref.at[:, pl.ds(pl.multiple_of(block * width, LANES), width)]
+
+
+def gather_all(g, own_ref, full, send_k, send_x, send_c, recv):
+    started = []
+
+    def put(src, block, sem, k, t):
+        copy = remote(src, cols(full, block), sem, recv.at[block], k, t)
+        copy.start()
+        started.append(copy)
+
+    def arrived(block):
+        remote(own_ref, cols(full, block), send_k.at[0], recv.at[block], g.kv, g.tp).wait_recv()
+
+    mine = g.block(g.kv, g.x, g.c)
+    for step in range(1, g.nk):
+        put(own_ref, mine, send_k.at[step], g.k(step), g.tp)
+    for dx in range(1, g.nx):
+        put(own_ref, mine, send_x.at[0, dx], g.kv, g.xi(dx) * CORES + g.c)
+    put(own_ref, mine, send_c.at[0, 0], g.kv, g.x * CORES + g.oc)
+    full[:, pl.ds(pl.multiple_of(mine * LANES, LANES), LANES)] = own_ref[...]
+
+    def cross(step):
+        k = g.k(g.nk - step)
+        for dx in range(1, g.nx):
+            block = g.block(k, g.xi(dx), g.c)
+            arrived(block)
+            put(cols(full, block), block, send_c.at[step, dx], g.kv, g.x * CORES + g.oc)
+
+    for step in range(1, g.nk):
+        block = g.block(g.k(g.nk - step), g.x, g.c)
+        arrived(block)
+        for dx in range(1, g.nx):
+            put(cols(full, block), block, send_x.at[step, dx], g.kv, g.xi(dx) * CORES + g.c)
+        put(cols(full, block), block, send_c.at[step, 0], g.kv, g.x * CORES + g.oc)
+        cross(step - 1)
+    cross(g.nk - 1)
+    for step in range(g.nk):
+        for dx in range(g.nx):
+            arrived(g.block(g.k(g.nk - step), g.xi(dx), g.oc))
+    for copy in started:
+        copy.wait_send()
+
+
+def hidden_units(full, gain_ref, wg, wu, acc_g, acc_u, hidden, width):
+    rows, depth = full.shape
+    acc_g[...] = jnp.zeros_like(acc_g)
+    acc_u[...] = jnp.zeros_like(acc_u)
+
+    def body(i, squares):
+        at = pl.ds(pl.multiple_of(i * width, LANES), width)
+        x = full[:, at].astype(F32)
+        u = (x * gain_ref[:, at]).astype(BF16)
+        acc_g[...] += jnp.dot(u, wg[at, :], preferred_element_type=F32)
+        acc_u[...] += jnp.dot(u, wu[at, :], preferred_element_type=F32)
+        return squares + jnp.sum(x * x, axis=1, keepdims=True)
+
+    squares = lax.fori_loop(0, depth // width, body, jnp.zeros((rows, 1), F32))
+    scale = lax.rsqrt(squares / depth + epsilon)
+    hidden[...] = (jax.nn.silu(scale * acc_g[...]) * (scale * acc_u[...])).astype(BF16)
+
+
+def down_scatter(g, hidden, wd, part, sib, out_x, in_x, keep, out_k, in_k, sa, ra, sb, rb, sc, rc):
+    width = g.nt * LANES
+    last = g.nk - 1
+
+    def kof(i):
+        return g.k(i + 1)
+
+    def copy_a(i, xx):
+        src = cols(part, g.block(kof(i), xx, g.oc))
+        return remote(src, sib.at[i, xx], sa.at[i, xx], ra.at[i, xx], g.kv, g.x * CORES + g.oc)
+
+    def copy_b(i, dx):
+        return remote(out_x.at[i, dx - 1], in_x.at[i, dx - 1], sb.at[i, dx - 1], rb.at[i, dx - 1], g.kv, g.xi(dx) * CORES + g.c)
+
+    def copy_c(i):
+        return remote(out_k.at[i], in_k.at[i], sc.at[i], rc.at[i], kof(i), g.tp)
+
+    def stage_a(i):
+        at = pl.ds(pl.multiple_of(kof(i) * width, LANES), width)
+        part[:, at] = jnp.dot(hidden[...], wd[:, at], preferred_element_type=F32).astype(BF16)
+        for xx in range(g.nx):
+            copy_a(i, xx).start()
+
+    def pair_sum(i, xx):
+        at = pl.ds(pl.multiple_of(g.block(kof(i), xx, g.c) * LANES, LANES), LANES)
+        return part[:, at].astype(F32) + sib[i, xx].astype(F32)
+
+    def stage_b(i):
+        for xx in range(g.nx):
+            copy_a(i, xx).wait_recv()
+        for dx in range(1, g.nx):
+            out_x[i, dx - 1] = pair_sum(i, g.xi(dx)).astype(BF16)
+            copy_b(i, dx).start()
+        keep[i % 2] = pair_sum(i, g.x)
+
+    def stage_c(i):
+        for dx in range(1, g.nx):
+            copy_b(i, dx).wait_recv()
+        total = keep[i % 2]
+        for dx in range(1, g.nx):
+            total = total + in_x[i, dx - 1].astype(F32)
+        return total
+
+    def send_c(i):
+        out_k[i] = stage_c(i).astype(BF16)
+        copy_c(i).start()
+
+    stage_a(0)
+    stage_a(1)
+    stage_b(0)
+
+    def body(i, carry):
+        stage_a(i)
+        send_c(i - 2)
+        stage_b(i - 1)
+        return carry
+
+    lax.fori_loop(2, g.nk, body, 0)
+    send_c(last - 1)
+    stage_b(last)
+    total = stage_c(last)
+    for i in range(last):
+        copy_c(i).wait_recv()
+        total = total + in_k[i].astype(F32)
+    for i in range(g.nk):
+        for xx in range(g.nx):
+            copy_a(i, xx).wait_send()
+        for dx in range(1, g.nx):
+            copy_b(i, dx).wait_send()
+        if i < last:
+            copy_c(i).wait_send()
+    return total
+
+
+def ff_scratch(nk, nt, rows, depth, units):
+    nx = nt // CORES
+    dma = pltpu.SemaphoreType.DMA
+    weights = [
+        pltpu.VMEM((depth, units), BF16),
+        pltpu.VMEM((depth, units), BF16),
+        pltpu.VMEM((units, depth), BF16),
+        dma((3,)),
+    ]
+    gather = [
+        pltpu.VMEM((rows, depth), BF16),
+        dma((nk,)),
+        dma((nk, nx)),
+        dma((nk, nx)),
+        dma((nk * nt,)),
+    ]
+    mid = [pltpu.VMEM((rows, units), F32), pltpu.VMEM((rows, units), F32), pltpu.VMEM((rows, units), BF16)]
+    scatter = [
+        pltpu.VMEM((rows, depth), BF16),
+        pltpu.VMEM((nk, nx, rows, LANES), BF16),
+        pltpu.VMEM((nk, nx - 1, rows, LANES), BF16),
+        pltpu.VMEM((nk, nx - 1, rows, LANES), BF16),
+        pltpu.VMEM((2, rows, LANES), F32),
+        pltpu.VMEM((nk - 1, rows, LANES), BF16),
+        pltpu.VMEM((nk - 1, rows, LANES), BF16),
+        dma((nk, nx)),
+        dma((nk, nx)),
+        dma((nk, nx - 1)),
+        dma((nk, nx - 1)),
+        dma((nk - 1,)),
+        dma((nk - 1,)),
+    ]
+    return weights + gather + mid + scatter
+
+
+N_FF = 4 + 5 + 3 + 13
+
+
+def load_weights(hbm, vmem, sem):
+    copies = [pltpu.make_async_copy(a, b, sem.at[i]) for i, (a, b) in enumerate(zip(hbm, vmem))]
+    for copy in copies:
+        copy.start()
+    return copies
+
+
+def run_ff(g, own_ref, gain_ref, loads, ff):
+    wg, wu, wd, _ = ff[:4]
+    full, send_k, send_x, send_c, recv = ff[4:9]
+    acc_g, acc_u, hidden = ff[9:12]
+    gather_all(g, own_ref, full, send_k, send_x, send_c, recv)
+    loads[0].wait()
+    loads[1].wait()
+    hidden_units(full, gain_ref, wg, wu, acc_g, acc_u, hidden, full.shape[1] // g.nk)
+    loads[2].wait()
+    total = down_scatter(g, hidden, wd, *ff[12:])
+    return own_ref[...].astype(F32) + 0.5 * total
+
+
+def first_kernel(nk, nt, tok, gain, mgain, wg_h, wu_h, wd_h, q_h, f_h, v_h, o_h, first, projected, *scratch):
+    g = Grid(nk, nt)
+    ff, rest = scratch[:N_FF], scratch[N_FF:]
+    mixw, mix_sem, block, bsend, brecv, normed, proj, got, sq, sq_got, psend, precv, qsend, qrecv = rest
+    loads = load_weights((wg_h, wu_h, wd_h), ff[:3], ff[3])
+    mix_loads = load_weights((q_h, f_h, v_h, o_h), [mixw.at[i] for i in range(4)], mix_sem)
+    barrier(g)
+    first[...] = run_ff(g, tok, gain, loads, ff).astype(BF16)
+
+    copies = []
+    for step in range(1, nt):
+        copy = remote(first, cols(block, g.tp), bsend.at[step - 1], brecv.at[step - 1], g.kv, g.t(step))
+        copy.start()
+        copies.append(copy)
+    block[:, pl.ds(pl.multiple_of(g.tp * LANES, LANES), LANES)] = first[...]
+    for step in range(1, nt):
+        src = g.t(nt - step)
+        remote(first, cols(block, src), bsend.at[step - 1], brecv.at[step - 1], g.kv, src).wait_recv()
+    width = block.shape[1]
+    x = block[...].astype(F32)
+    normed[...] = (x * mgain[:, pl.ds(pl.multiple_of(g.kv * width, LANES), width)]).astype(BF16)
+    sq[...] = jnp.broadcast_to(jnp.sum(x * x, axis=1, keepdims=True), sq.shape)
+    own_rows, inner = projected.shape[0], projected.shape[1] // 4
+
+    def rows_of(k):
+        return pl.ds(pl.multiple_of(k * own_rows, own_rows), own_rows)
+
+    def q_copy(step):
+        return remote(sq.at[rows_of(g.k(step))], sq_got.at[step - 1], qsend.at[step - 1], qrecv.at[step - 1], g.k(step), g.tp)
+
+    def p_copy(i, step):
+        return remote(
+            proj.at[i, rows_of(g.k(step))], got.at[i, step - 1], psend.at[i, step - 1], precv.at[i, step - 1], g.k(step), g.tp
+        )
+
+    for step in range(1, nk):
+        q_copy(step).start()
+    for i in range(4):
+        mix_loads[i].wait()
+        proj[i] = jnp.dot(normed[...], mixw[i], preferred_element_type=F32).astype(BF16)
+        for step in range(1, nk):
+            p_copy(i, step).start()
+    squares = sq[rows_of(g.kv), :]
+    for step in range(1, nk):
+        q_copy(step).wait_recv()
+        squares = squares + sq_got[step - 1]
+    scale = lax.rsqrt(squares[:, :1] / mgain.shape[1] + epsilon)
+    for i in range(4):
+        total = proj[i, rows_of(g.kv), :].astype(F32)
+        for step in range(1, nk):
+            p_copy(i, step).wait_recv()
+            total = total + got[i, step - 1].astype(F32)
+        projected[:, i * inner : (i + 1) * inner] = total * scale
+    for copy in copies:
+        copy.wait_send()
+    for step in range(1, nk):
+        q_copy(step).wait_send()
+        for i in range(4):
+            p_copy(i, step).wait_send()
+
+
+def second_kernel(nk, nt, y, first, gain, po_h, wg_h, wu_h, wd_h, result, *scratch):
+    g = Grid(nk, nt)
+    ff, rest = scratch[:N_FF], scratch[N_FF:]
+    po, po_sem, yfull, ysend, yrecv, part, got, tsend, trecv, second = rest
+    po_load = load_weights((po_h,), (po,), po_sem)
+    loads = load_weights((wg_h, wu_h, wd_h), ff[:3], ff[3])
+    barrier(g)
+    own_rows = y.shape[0]
+
+    def rows_of(k):
+        return pl.ds(pl.multiple_of(k * own_rows, own_rows), own_rows)
+
+    def y_copy(step, k, src):
+        return remote(y, yfull.at[rows_of(src)], ysend.at[step - 1], yrecv.at[step - 1], k, g.tp)
+
+    for step in range(1, nk):
+        y_copy(step, g.k(step), g.kv).start()
+    yfull[rows_of(g.kv), :] = y[...]
+    for step in range(1, nk):
+        y_copy(step, g.k(step), g.k(nk - step)).wait_recv()
+    po_load[0].wait()
+    part[...] = jnp.dot(yfull[...], po[...], preferred_element_type=F32).astype(BF16)
+
+    def t_copy(step):
+        return remote(cols(part, g.t(step)), got.at[step - 1], tsend.at[step - 1], trecv.at[step - 1], g.kv, g.t(step))
+
+    for step in range(1, nt):
+        t_copy(step).start()
+    total = part[:, pl.ds(pl.multiple_of(g.tp * LANES, LANES), LANES)].astype(F32)
+    for step in range(1, nt):
+        t_copy(step).wait_recv()
+        total = total + got[step - 1].astype(F32)
+    second[...] = (first[...].astype(F32) + total).astype(BF16)
+    result[...] = run_ff(g, second, gain, loads, ff).astype(BF16)
+    for step in range(1, nk):
+        y_copy(step, g.k(step), g.kv).wait_send()
+    for step in range(1, nt):
+        t_copy(step).wait_send()
+
+
+def call(kernel, ident, outs, n_vmem, n_any, scratch, args):
+    vmem, any_space = pl.BlockSpec(memory_space=pltpu.VMEM), pl.BlockSpec(memory_space=pl.ANY)
+    return pl.pallas_call(
+        kernel,
+        out_shape=outs,
+        in_specs=[vmem] * n_vmem + [any_space] * n_any,
+        out_specs=jax.tree.map(lambda _: vmem, outs),
+        scratch_shapes=scratch,
+        compiler_params=pltpu.CompilerParams(
+            collective_id=ident, has_side_effects=True, vmem_limit_bytes=56 * 1024 * 1024
+        ),
+    )(*args)
+
+
+def per_device(
+    tokens, past_state, pre_gain, pre_gate, pre_up, pre_down, mix_gain,
+    query_weight, forget_weight, value_weight, output_gate_weight,
+    forget_floor, head_gain, proj_out, post_gain, post_gate, post_up, post_down,
+):
+    nk, nt = lax.axis_size("kv"), lax.axis_size("tp")
+    rows, depth, units = tokens.shape[0], pre_gate.shape[0], pre_gate.shape[1]
+    own_rows, local_heads, head_width = past_state.shape[:3]
+    inner = local_heads * head_width
+    width = query_weight.shape[0]
+    dma = pltpu.SemaphoreType.DMA
+    base = ff_scratch(nk, nt, rows, depth, units)
+    first, projected = call(
+        functools.partial(first_kernel, nk, nt),
+        0,
+        (jax.ShapeDtypeStruct(tokens.shape, BF16), jax.ShapeDtypeStruct((own_rows, 4 * inner), F32)),
+        3,
+        7,
+        base
+        + [
+            pltpu.VMEM((4, width, inner), BF16),
+            dma((4,)),
+            pltpu.VMEM((rows, width), BF16),
+            dma((nt - 1,)),
+            dma((nt - 1,)),
+            pltpu.VMEM((rows, width), BF16),
+            pltpu.VMEM((4, rows, inner), BF16),
+            pltpu.VMEM((4, nk - 1, own_rows, inner), BF16),
+            pltpu.VMEM((rows, LANES), F32),
+            pltpu.VMEM((nk - 1, own_rows, LANES), F32),
+            dma((4, nk - 1)),
+            dma((4, nk - 1)),
+            dma((nk - 1,)),
+            dma((nk - 1,)),
+        ],
+        (
+            tokens, pre_gain[None], mix_gain[None], pre_gate, pre_up, pre_down,
+            query_weight, forget_weight, value_weight, output_gate_weight,
+        ),
+    )
+    pre_query, pre_forget, pre_value, pre_gate_out = jnp.split(projected, 4, axis=1)
+    head_shape = (own_rows, local_heads, head_width)
+    floors = forget_floor.reshape(local_heads, head_width)
+    forget_heads = pre_forget.reshape(head_shape)
+    forget = floors + (1.0 - floors) * jax.nn.sigmoid(forget_heads)
+    written = (1.0 - floors) * jax.nn.sigmoid(-forget_heads)
+    query_act = jax.nn.silu(pre_query.reshape(head_shape))
+    value_act = pre_value.reshape(head_shape)
+    new_state = (
+        forget[:, :, :, None] * past_state + written[:, :, :, None] * value_act[:, :, None, :]
+    )
+    readout = jnp.einsum("bhkv,bhk->bhv", new_state, query_act, precision=lax.Precision.HIGHEST)
+    readout = (
+        readout
+        * lax.rsqrt(jnp.mean(readout * readout, axis=2, keepdims=True) + epsilon)
+        * head_gain
+    )
+    mixed_in = (readout.reshape(own_rows, inner) * jax.nn.silu(pre_gate_out)).astype(BF16)
+    result = call(
+        functools.partial(second_kernel, nk, nt),
+        1,
+        jax.ShapeDtypeStruct(tokens.shape, BF16),
+        3,
+        4,
+        base
+        + [
+            pltpu.VMEM(proj_out.shape, BF16),
+            dma((1,)),
+            pltpu.VMEM((rows, inner), BF16),
+            dma((nk - 1,)),
+            dma((nk - 1,)),
+            pltpu.VMEM((rows, width), BF16),
+            pltpu.VMEM((nt - 1, rows, LANES), BF16),
+            dma((nt - 1,)),
+            dma((nt - 1,)),
+            pltpu.VMEM((rows, LANES), BF16),
+        ],
+        (mixed_in, first, post_gain[None], proj_out, post_gate, post_up, post_down),
+    )
+    return (result, new_state)
+
+
 def solution(mesh):
     placed = (
         P(None, ("kv", "tp")),
@@ -153,8 +591,9 @@
         P(None, ("kv", "tp")),
         P(("kv", "tp"), None),
     )
+    blocks_fit = D == mesh.shape["kv"] * mesh.shape["tp"] * LANES and mesh.shape["tp"] >= 2 * CORES
     return jax.shard_map(
-        per_device,
+        per_device if blocks_fit else per_device_plain,
         mesh=mesh,
         in_specs=placed,
         out_specs=(P(None, ("kv", "tp")), P("kv", "tp", None, None)),

time: 550 us -> 209 us (0.38)
  waiting for transfers between devices: 418 us -> 0 us
  Pallas kernels: 0 us -> 166 us
  blocking collectives: 52.4 us -> 0 us
  matrix products: 36.1 us -> 9.6 us
  between operations: 14.4 us -> 0.76 us
  local copies, waits for them, and re-layouts: 6.21 us -> 18.1 us
  other arithmetic: 20.7 us -> 13.2 us
    reduce_scatter x3 -> x0, waiting for transfers between devices: 253 us -> none  [the longest x1 142 us: down_sum(): lax.psum_scatter(jnp.dot(hidden, w_down, preferred_element_type=jnp.float...]
    pallas_call x0 -> x2, Pallas kernels: none -> 166 us  [call(): pl.pallas_call(kernel, out_shape=outs, in_specs=[vmem] * n_vmem + [any_sp...]
    all_gather x2 -> x0, waiting for transfers between devices: 113 us -> none  [the longest x1 58.6 us: per_device(): whole_rows = lax.all_gather(tokens, ('kv', 'tp'), axis=1, tiled=True)]
    psum x1 -> x0, waiting for transfers between devices: 32.8 us -> none  [per_device(): block_sum = lax.psum(kv_sums, 'tp').astype(jnp.float32)]
    all_gather x1 -> x0, blocking collectives: 30.8 us -> none  [per_device(): lax.all_gather(mixed_in, 'kv', axis=0, tiled=True)]
    dot_general x9 -> x0, matrix products: 28.9 us -> none  [the longest x1 8.94 us: down_sum(): jnp.dot(hidden, w_down, preferred_element_type=jnp.float32)]
    psum x1 -> x0, blocking collectives: 21.6 us -> none  [per_device(): squares = lax.psum(jnp.sum(block_float * block_float, axis=1), 'kv')]
    unnamed x8 -> x0, waiting for transfers between devices: 19.9 us -> none
  transfers between devices with their start and end apart: 7 -> 0, of which waited for: 7 -> 0; matrix products, arithmetic and copies ran while one was open for 0% -> 0% of each run, Pallas kernels for 0% -> 0%
where the time goes in v1:
time: 209 us; the launch traced here: 207 us
  Pallas kernels  166 us (79%)
  local copies, waits for them, and re-layouts  18.1 us (9%)
  other arithmetic  13.2 us (6%)
  matrix products  9.6 us (5%)
    pallas_call x2, Pallas kernels, call(): pl.pallas_call(kernel, out_shape=outs, in_specs=[vmem] * n_vmem + [any_sp...  166 us
    unnamed x13, local copies, waits for them, and re-layouts  18 us
    add x1, other arithmetic, per_device(): forget[:, :, :, None] * past_state  10.5 us
    dot_general x1, matrix products, per_device(): jnp.einsum('bhkv,bhk->bhv', new_state, query_act, precision=lax.Precision...  9.6 us

profile of v1, /device:TPU:0, one launch (start us, length us, event | category | flops | bytes accessed | tf_op | source)
XLA Modules:
  0.0 207.4 jit_solution(9821150657559963852)
XLA Ops:
  0.6 4.6 %copy.20.wg_h = bf16[4096,352]{1,0:T(8,128)(2,1)} copy(bf16[4096,352]{0,1:T(8,128)(2,1)} %param.21) | data formatting | bytes 5767168 | tf_op args[3]
  5.2 0.0 copy-start.1
  5.2 4.6 %copy.21.wu_h = bf16[4096,352]{1,0:T(8,128)(2,1)} copy(bf16[4096,352]{0,1:T(8,128)(2,1)} %param.22) | data formatting | bytes 5767168 | tf_op args[4]
  9.8 95.1 %shard_map.185 = (bf16[256,128]{1,0:T(8,128)(2,1)}, f32[32,2048]{1,0:T(8,128)}) custom-call(bf16[256,128]{1,0:T(8,128)(2,1)} %tok.1, f32[1,4096]{1,0:T(1,128)} %bitcast.31, f32[1,4096]{1,0:T(1,128)} %bitcast.32, bf16[4096,352]{1,0:T(8,128)(2,1)} %copy.20.wg_h, bf16[4096,352]{1,0:T(8,128)(2,1)} %copy.21.wu_h, bf16[352,4096]{1,0:T(8,128)(2,1)} %wd_h.2, ...), custom_call_target="tpu_custom_call" | custom-call | tf_op jit(solution)/shard_map/pallas_call | solution.py:479
  104.9 1.0 fusion.1
  105.9 0.0 copy-done.1
  106.0 10.5 %multiply_add_fusion = f32[32,4,128,128]{3,2,1,0:T(8,128)} fusion(f32[32,4,128,128]{3,2,1,0:T(8,128)} %param.19, f32[32,4,128]{2,1,0:T(4,128)S(1)} %mul.81, f32[32,4,128]{2,1,0:T(4,128)S(1)} %bitcast.27, f32[32,4,128]{2,1,0:T(4,128)S(1)} %bitcast.26), kind=kLoop, calls=%fused_computation | loop fusion | flops 6291456 | bytes 16973824 | tf_op jit(solution)/shard_map/add | solution.py:540
  116.5 0.0 copy-start.2
  116.5 0.0 copy-start
  116.6 9.6 %fusion.2 = f32[32,4,1,128]{3,2,1,0:T(1,128)S(1)} fusion(f32[32,4,128,128]{3,2,1,0:T(8,128)} %multiply_add_fusion, f32[32,4,128,1]{2,3,1,0:T(1,128)S(1)} %bitcast.25), kind=kOutput, calls=%fused_computation.13 | convolution fusion | flops 25165824 | bytes 8519680 | tf_op jit(solution)/shard_map/bhkv,bhk->bhv/dot_general | solution.py:542
  126.2 0.1 multiply_reduce_fusion
  126.3 0.0 copy-done.2
  126.3 0.1 multiply_multiply_fusion
  126.5 1.5 fusion.y
  127.9 0.0 copy-done
  127.9 2.8 %copy.22.wg_h = bf16[4096,352]{1,0:T(8,128)(2,1)} copy(bf16[4096,352]{0,1:T(8,128)(2,1)S(1)} %copy-done) | data formatting | bytes 5767168 | tf_op args[15]
  130.7 4.6 %copy.23.wu_h = bf16[4096,352]{1,0:T(8,128)(2,1)} copy(bf16[4096,352]{0,1:T(8,128)(2,1)} %param.34) | data formatting | bytes 5767168 | tf_op args[16]
  135.3 70.6 %shard_map.186 = bf16[256,128]{1,0:T(8,128)(2,1)} custom-call(bf16[32,512]{1,0:T(8,128)(2,1)} %fusion.y, bf16[256,128]{1,0:T(8,128)(2,1)} %get-tuple-element.5.first, f32[1,4096]{1,0:T(1,128)} %bitcast.33, bf16[512,512]{1,0:T(8,128)(2,1)} %po_h.1, bf16[4096,352]{1,0:T(8,128)(2,1)} %copy.22.wg_h, bf16[4096,352]{1,0:T(8,128)(2,1)} %copy.23.wu_h, ...), custom_call_target="tpu_custom_call" | custom-call | tf_op jit(solution)/shard_map/pallas_call | solution.py:479
  205.9 1.5 copy.29
  (10 shorter events, 0.2 us)
Async XLA Ops:
  5.2 100.7 %copy-start.1 = (f32[512]{0:T(512)S(1)}, f32[512]{0:T(512)}, u32[]{:S(2)}) copy-start(f32[512]{0:T(512)} %param.29) | copy-start | bytes 6148
  116.5 9.8 %copy-start.2 = (f32[128]{0:T(128)S(1)}, f32[128]{0:T(128)}, u32[]{:S(2)}) copy-start(f32[128]{0:T(128)} %param.30) | copy-start | bytes 1540
  116.5 11.4 %copy-start = (bf16[4096,352]{0,1:T(8,128)(2,1)S(1)}, bf16[4096,352]{0,1:T(8,128)(2,1)}, u32[]{:S(2)}) copy-start(bf16[4096,352]{0,1:T(8,128)(2,1)} %param.33) | copy-start | bytes 8650756

commit v2 on v1

--- a/solution.py
+++ b/solution.py
@@ -137,6 +137,7 @@
 
 
 LANES = 128
+LAST = (((1,), (1,)), ((), ()))
 CORES = 2
 F32, BF16 = jnp.float32, jnp.bfloat16
 MESH = pl.DeviceIdType.MESH
@@ -232,8 +233,8 @@
         at = pl.ds(pl.multiple_of(i * width, LANES), width)
         x = full[:, at].astype(F32)
         u = (x * gain_ref[:, at]).astype(BF16)
-        acc_g[...] += jnp.dot(u, wg[at, :], preferred_element_type=F32)
-        acc_u[...] += jnp.dot(u, wu[at, :], preferred_element_type=F32)
+        acc_g[...] += lax.dot_general(u, wg[:, at], LAST, preferred_element_type=F32)
+        acc_u[...] += lax.dot_general(u, wu[:, at], LAST, preferred_element_type=F32)
         return squares + jnp.sum(x * x, axis=1, keepdims=True)
 
     squares = lax.fori_loop(0, depth // width, body, jnp.zeros((rows, 1), F32))
@@ -319,8 +320,8 @@
     nx = nt // CORES
     dma = pltpu.SemaphoreType.DMA
     weights = [
-        pltpu.VMEM((depth, units), BF16),
-        pltpu.VMEM((depth, units), BF16),
+        pltpu.VMEM((units, depth), BF16),
+        pltpu.VMEM((units, depth), BF16),
         pltpu.VMEM((units, depth), BF16),
         dma((3,)),
     ]
@@ -376,7 +377,7 @@
 def first_kernel(nk, nt, tok, gain, mgain, wg_h, wu_h, wd_h, q_h, f_h, v_h, o_h, first, projected, *scratch):
     g = Grid(nk, nt)
     ff, rest = scratch[:N_FF], scratch[N_FF:]
-    mixw, mix_sem, block, bsend, brecv, normed, proj, got, sq, sq_got, psend, precv, qsend, qrecv = rest
+    mixw, mix_sem, block, bsend, brecv, normed, proj, mate_got, sums, got, sq, sq_got, msend, mrecv, psend, precv, qsend, qrecv = rest
     loads = load_weights((wg_h, wu_h, wd_h), ff[:3], ff[3])
     mix_loads = load_weights((q_h, f_h, v_h, o_h), [mixw.at[i] for i in range(4)], mix_sem)
     barrier(g)
@@ -403,35 +404,105 @@
     def q_copy(step):
         return remote(sq.at[rows_of(g.k(step))], sq_got.at[step - 1], qsend.at[step - 1], qrecv.at[step - 1], g.k(step), g.tp)
 
-    def p_copy(i, step):
-        return remote(
-            proj.at[i, rows_of(g.k(step))], got.at[i, step - 1], psend.at[i, step - 1], precv.at[i, step - 1], g.k(step), g.tp
-        )
+    nz, z, y = nk // 2, g.kv // 2, g.kv % 2
+
+    def zi(dz):
+        return lax.rem(z + dz, nz)
+
+    def m_copy(i, dz):
+        src = proj.at[i, zi(dz) * 2 + 1 - y]
+        return remote(src, mate_got.at[i, dz], msend.at[i, dz], mrecv.at[i, dz], 2 * z + 1 - y, g.tp)
+
+    def p_copy(i, dz):
+        at = dz - 1
+        return remote(sums.at[i, at], got.at[i, at], psend.at[i, at], precv.at[i, at], zi(dz) * 2 + y, g.tp)
+
+    def mate_sum(i, dz):
+        m_copy(i, dz).wait_recv()
+        return proj[i, zi(dz) * 2 + y].astype(F32) + mate_got[i, dz].astype(F32)
+
+    def forward(i):
+        for dz in range(1, nz):
+            sums[i, dz - 1] = mate_sum(i, dz).astype(BF16)
+            p_copy(i, dz).start()
 
     for step in range(1, nk):
         q_copy(step).start()
     for i in range(4):
         mix_loads[i].wait()
-        proj[i] = jnp.dot(normed[...], mixw[i], preferred_element_type=F32).astype(BF16)
-        for step in range(1, nk):
-            p_copy(i, step).start()
+        out = jnp.dot(normed[...], mixw[i], preferred_element_type=F32).astype(BF16)
+        proj[i] = out.reshape(nk, own_rows, inner)
+        for dz in range(1, nz + 1):
+            m_copy(i, dz % nz).start()
+        if i:
+            forward(i - 1)
+    forward(3)
     squares = sq[rows_of(g.kv), :]
     for step in range(1, nk):
         q_copy(step).wait_recv()
         squares = squares + sq_got[step - 1]
     scale = lax.rsqrt(squares[:, :1] / mgain.shape[1] + epsilon)
     for i in range(4):
-        total = proj[i, rows_of(g.kv), :].astype(F32)
-        for step in range(1, nk):
-            p_copy(i, step).wait_recv()
-            total = total + got[i, step - 1].astype(F32)
+        total = mate_sum(i, 0)
+        for dz in range(1, nz):
+            p_copy(i, dz).wait_recv()
+            total = total + got[i, dz - 1].astype(F32)
         projected[:, i * inner : (i + 1) * inner] = total * scale
     for copy in copies:
         copy.wait_send()
     for step in range(1, nk):
         q_copy(step).wait_send()
-        for i in range(4):
-            p_copy(i, step).wait_send()
+    for i in range(4):
+        for dz in range(nz):
+            m_copy(i, dz).wait_send()
+        for dz in range(1, nz):
+            p_copy(i, dz).wait_send()
+
+
+def recurrence_kernel(projected, past, floor, head_gain, new, mixed):
+    rows, heads, width = past.shape[:3]
+    inner = heads * width
+    for h in range(heads):
+        def part(i):
+            return projected[:, i * inner + h * width : i * inner + (h + 1) * width]
+
+        at = slice(h * width, (h + 1) * width)
+        base = floor[:, at]
+        forget = (base + (1.0 - base) * jax.nn.sigmoid(part(1))).T
+        written = ((1.0 - base) * jax.nn.sigmoid(-part(1))).T
+        query = jax.nn.silu(part(0)).T
+        value = part(2)
+        outs = []
+        for n in range(rows):
+            col = slice(n, n + 1)
+            state = forget[:, col] * past[n, h] + written[:, col] * value[col]
+            new[n, h] = state
+            outs.append(jnp.sum(state * query[:, col], axis=0, keepdims=True))
+        read = jnp.concatenate(outs, axis=0)
+        read = read * lax.rsqrt(jnp.mean(read * read, axis=1, keepdims=True) + epsilon) * head_gain[...]
+        mixed[:, at] = (read * jax.nn.silu(part(3))).astype(BF16)
+
+
+def recurrence(projected, past_state, forget_floor, head_gain):
+    rows, heads, width = past_state.shape[:3]
+    inner, step = heads * width, 8
+    state_spec = pl.BlockSpec((step, heads, width, width), lambda i: (i, 0, 0, 0))
+    return pl.pallas_call(
+        recurrence_kernel,
+        grid=(rows // step,),
+        out_shape=(
+            jax.ShapeDtypeStruct(past_state.shape, F32),
+            jax.ShapeDtypeStruct((rows, inner), BF16),
+        ),
+        in_specs=[
+            pl.BlockSpec((step, 4 * inner), lambda i: (i, 0)),
+            state_spec,
+            pl.BlockSpec((1, inner), lambda i: (0, 0)),
+            pl.BlockSpec((1, width), lambda i: (0, 0)),
+        ],
+        out_specs=(state_spec, pl.BlockSpec((step, inner), lambda i: (i, 0))),
+        compiler_params=pltpu.CompilerParams(vmem_limit_bytes=32 * 1024 * 1024),
+    )(projected, past_state, forget_floor[None], head_gain[None])
 
 
 def second_kernel(nk, nt, y, first, gain, po_h, wg_h, wu_h, wd_h, result, *scratch):
@@ -514,38 +585,25 @@
             dma((nt - 1,)),
             dma((nt - 1,)),
             pltpu.VMEM((rows, width), BF16),
-            pltpu.VMEM((4, rows, inner), BF16),
-            pltpu.VMEM((4, nk - 1, own_rows, inner), BF16),
+            pltpu.VMEM((4, nk, own_rows, inner), BF16),
+            pltpu.VMEM((4, nk // 2, own_rows, inner), BF16),
+            pltpu.VMEM((4, nk // 2 - 1, own_rows, inner), BF16),
+            pltpu.VMEM((4, nk // 2 - 1, own_rows, inner), BF16),
             pltpu.VMEM((rows, LANES), F32),
             pltpu.VMEM((nk - 1, own_rows, LANES), F32),
-            dma((4, nk - 1)),
-            dma((4, nk - 1)),
+            dma((4, nk // 2)),
+            dma((4, nk // 2)),
+            dma((4, nk // 2 - 1)),
+            dma((4, nk // 2 - 1)),
             dma((nk - 1,)),
             dma((nk - 1,)),
         ],
         (
-            tokens, pre_gain[None], mix_gain[None], pre_gate, pre_up, pre_down,
+            tokens, pre_gain[None], mix_gain[None], pre_gate.T, pre_up.T, pre_down,
             query_weight, forget_weight, value_weight, output_gate_weight,
         ),
     )
-    pre_query, pre_forget, pre_value, pre_gate_out = jnp.split(projected, 4, axis=1)
-    head_shape = (own_rows, local_heads, head_width)
-    floors = forget_floor.reshape(local_heads, head_width)
-    forget_heads = pre_forget.reshape(head_shape)
-    forget = floors + (1.0 - floors) * jax.nn.sigmoid(forget_heads)
-    written = (1.0 - floors) * jax.nn.sigmoid(-forget_heads)
-    query_act = jax.nn.silu(pre_query.reshape(head_shape))
-    value_act = pre_value.reshape(head_shape)
-    new_state = (
-        forget[:, :, :, None] * past_state + written[:, :, :, None] * value_act[:, :, None, :]
-    )
-    readout = jnp.einsum("bhkv,bhk->bhv", new_state, query_act, precision=lax.Precision.HIGHEST)
-    readout = (
-        readout
-        * lax.rsqrt(jnp.mean(readout * readout, axis=2, keepdims=True) + epsilon)
-        * head_gain
-    )
-    mixed_in = (readout.reshape(own_rows, inner) * jax.nn.silu(pre_gate_out)).astype(BF16)
+    new_state, mixed_in = recurrence(projected, past_state, forget_floor, head_gain)
     result = call(
         functools.partial(second_kernel, nk, nt),
         1,
@@ -565,7 +623,7 @@
             dma((nt - 1,)),
             pltpu.VMEM((rows, LANES), BF16),
         ],
-        (mixed_in, first, post_gain[None], proj_out, post_gate, post_up, post_down),
+        (mixed_in, first, post_gain[None], proj_out, post_gate.T, post_up.T, post_down),
     )
     return (result, new_state)
 

time: 209 us -> 174 us (0.83)
  other arithmetic: 13.2 us -> 0 us
  local copies, waits for them, and re-layouts: 18.1 us -> 6.42 us
  matrix products: 9.6 us -> 0 us
    unnamed x13 -> x11, local copies, waits for them, and re-layouts: 18 us -> 6.42 us
    pallas_call x0 -> x1, Pallas kernels: none -> 10.7 us  [recurrence(): pl.pallas_call(recurrence_kernel, grid=(rows // step,), out_shape=(jax.Sh...]
    pallas_call x2, Pallas kernels: 166 us -> 155 us  [call(): pl.pallas_call(kernel, out_shape=outs, in_specs=[vmem] * n_vmem + [any_sp...]
    add x2 -> x0, other arithmetic: 10.5 us -> none  [the longest x1 10.5 us: per_device(): forget[:, :, :, None] * past_state]
    dot_general x1 -> x0, matrix products: 9.6 us -> none  [per_device(): jnp.einsum('bhkv,bhk->bhv', new_state, query_act, precision=lax.Precision...]
where the time goes in v2:
time: 174 us; the launch traced here: 173 us
  Pallas kernels  166 us (95%)
  local copies, waits for them, and re-layouts  6.42 us (4%)
    pallas_call x2, Pallas kernels, call(): pl.pallas_call(kernel, out_shape=outs, in_specs=[vmem] * n_vmem + [any_sp...  155 us
    pallas_call x1, Pallas kernels, recurrence(): pl.pallas_call(recurrence_kernel, grid=(rows // step,), out_shape=(jax.Sh...  10.7 us
    unnamed x11, local copies, waits for them, and re-layouts  6.42 us

profile of v2, /device:TPU:0, one launch (start us, length us, event | category | flops | bytes accessed | tf_op | source)
XLA Modules:
  0.0 172.9 jit_solution(11028492370589761908)
XLA Ops:
  0.6 0.0 copy-start.3
  0.6 0.0 copy-start.4
  0.7 86.0 %shard_map.185 = (bf16[256,128]{1,0:T(8,128)(2,1)}, f32[32,2048]{1,0:T(8,128)}) custom-call(bf16[256,128]{1,0:T(8,128)(2,1)} %tok.1, f32[1,4096]{1,0:T(1,128)} %bitcast.15, f32[1,4096]{1,0:T(1,128)} %bitcast.16, bf16[352,4096]{1,0:T(8,128)(2,1)} %bitcast.11, bf16[352,4096]{1,0:T(8,128)(2,1)} %bitcast.12, bf16[352,4096]{1,0:T(8,128)(2,1)} %wd_h.2, ...), custom_call_target="tpu_custom_call" | custom-call | tf_op jit(solution)/shard_map/pallas_call | solution.py:550
  86.7 0.0 copy-done.3
  86.7 0.0 copy-done.4
  86.7 0.0 copy-start
  86.7 3.4 %copy-done = f32[32,4,128,128]{3,2,1,0:T(8,128)S(1)} copy-done((f32[32,4,128,128]{3,2,1,0:T(8,128)S(1)}, f32[32,4,128,128]{3,2,1,0:T(8,128)}, u32[]{:S(2)}) %copy-start) | copy-done | bytes 8388632
  90.1 0.0 copy-start.1
  90.1 0.9 copy-done.1
  91.0 10.7 %shard_map.186 = (f32[32,4,128,128]{3,2,1,0:T(8,128)}, bf16[32,512]{1,0:T(8,128)(2,1)S(1)}) custom-call(f32[32,2048]{1,0:T(8,128)S(1)} %copy-done.1, f32[32,4,128,128]{3,2,1,0:T(8,128)S(1)} %copy-done, f32[1,512]{1,0:T(1,128)S(1)} %bitcast.9, f32[1,128]{1,0:T(1,128)S(1)} %bitcast.10), custom_call_target="tpu_custom_call" | custom-call | tf_op jit(solution)/shard_map/pallas_call | solution.py:490
  101.7 0.0 copy-start.2
  101.7 0.6 copy-done.2
  102.3 69.1 %shard_map.187 = bf16[256,128]{1,0:T(8,128)(2,1)} custom-call(bf16[32,512]{1,0:T(8,128)(2,1)} %copy-done.2, bf16[256,128]{1,0:T(8,128)(2,1)} %get-tuple-element.8.first, f32[1,4096]{1,0:T(1,128)} %bitcast.17, bf16[512,512]{1,0:T(8,128)(2,1)} %po_h.1, bf16[352,4096]{1,0:T(8,128)(2,1)} %bitcast.13, bf16[352,4096]{1,0:T(8,128)(2,1)} %bitcast.14, ...), custom_call_target="tpu_custom_call" | custom-call | tf_op jit(solution)/shard_map/pallas_call | solution.py:550
  171.4 1.5 copy.21
Async XLA Ops:
  0.6 86.0 %copy-start.3 = (f32[512]{0:T(512)S(1)}, f32[512]{0:T(512)}, u32[]{:S(2)}) copy-start(f32[512]{0:T(512)} %param.29) | copy-start | bytes 6148
  0.6 86.0 %copy-start.4 = (f32[128]{0:T(128)S(1)}, f32[128]{0:T(128)}, u32[]{:S(2)}) copy-start(f32[128]{0:T(128)} %param.30) | copy-start | bytes 1540
  86.7 3.4 %copy-start = (f32[32,4,128,128]{3,2,1,0:T(8,128)S(1)}, f32[32,4,128,128]{3,2,1,0:T(8,128)}, u32[]{:S(2)}) copy-start(f32[32,4,128,128]{3,2,1,0:T(8,128)} %past.1) | copy-start | bytes 25165828
  90.1 0.9 copy-start.1
  101.7 0.6 copy-start.2
